TPU v7x, 32 devices: a whole 2x2x4 slice. The times are simulated.
32 devices in a mesh: fs: 4 (over z), tp: 4 (over y, x), rep: 2 (over core).
Axes of the slice: x: 2, y: 2, z: 4, core: 2. Of those that a mesh axis runs over, the one named last changes fastest.
Arguments:
- grads: float32 [2, 2, 8192, 2048], P('rep', None, 'fs', 'tp'), may hold values from -50 to 50
- momentum: float32 [2, 8192, 2048], P('rep', 'fs', 'tp'), may hold values from -14 to 14
Outputs:
- new_momentum: float32 [2, 8192, 2048], P('rep', 'fs', 'tp')
- step_matrix: float32 [2, 8192, 2048], P('rep', 'fs', 'tp')
All inputs are finite; a program needn't handle non-finite values.
Results may differ from a plain program's by a relative error of at most 0.0003.
Values sent between devices are 32-bit elements; how exact they have to be, the bound alone decides.
A program may use at most 128 MiB of HBM per device.

v0:
```python
import math

import jax
import jax.numpy as jnp
from jax import lax
from jax.sharding import PartitionSpec as P

ITERS = 3

momentum_decay = 0.95
norm_spread = 2.56
poly_linear = 3.4445
poly_cubic = -4.775
poly_quintic = 2.0315


def mul(a, b, contract=((1,), (0,)), precision=lax.Precision.HIGHEST):
    return lax.dot_general(
        a,
        b,
        (contract, ((), ())),
        precision=precision,
        preferred_element_type=jnp.float32,
    )


def own_share(panel, place, count):
    width = panel.shape[1]
    half = width // 2
    blocks = [
        lax.dynamic_slice_in_dim(panel, lax.rem(place + step, count) * width, width, 0)
        for step in range(count // 2 + 1)
    ]
    far = blocks[-1]
    far = jnp.where(place < count // 2, far[:half], far[:, half:].T)
    return jnp.concatenate(blocks[:-1] + [far], axis=0)


def gather_shares(share):
    return lax.all_gather(share, "tp", axis=0, tiled=False)


def whole_matrix(shares):
    count, width = shares.shape[0], shares.shape[2]
    middle = count // 2
    matrix = jnp.zeros((count * width, count * width), jnp.float32)

    def block(row, col):
        step = (row - col) % count
        if step < middle:
            return shares[col, step * width : (step + 1) * width]
        if step == middle and row > col:
            return jnp.concatenate(
                [shares[col, middle * width :], shares[row, middle * width :]], axis=0
            )
        return block(col, row).T

    for row in range(count):
        for col in range(count):
            matrix = lax.dynamic_update_slice(
                matrix, block(row, col), (row * width, col * width)
            )
    return matrix


def gram_share(gathered, place, count):
    size = gathered.shape[1]
    width = size // count
    half = width // 2
    rows = ((0,), (0,))

    def columns(begin, length):
        return lax.dynamic_slice_in_dim(gathered, begin, length, 1)

    own = columns(place * width, width)
    terms = [
        mul(columns(lax.rem(place + step, count) * width, width), own, rows)
        for step in range(count // 2)
    ]
    other = lax.rem(place + count // 2, count)
    high, low = jnp.maximum(place, other), jnp.minimum(place, other)
    begin = high * width + jnp.where(place < count // 2, 0, half)
    terms.append(mul(columns(begin, half), columns(low * width, width), rows))
    return jnp.concatenate(terms, axis=0)


def orthogonalize(moment):
    count = lax.axis_size("tp")
    place = lax.axis_index("tp")
    gathered = lax.all_gather(moment, "tp", axis=1, tiled=True)
    size = gathered.shape[1]
    width = size // count
    share = lax.psum_scatter(
        gram_share(gathered, place, count), "fs", scatter_dimension=0, tiled=True
    )
    share = lax.all_gather(share, "fs", axis=0, tiled=True)
    shares = gather_shares(share)
    on_diagonal = lax.broadcasted_iota(
        jnp.int32, (count, width, width), 1
    ) == lax.broadcasted_iota(jnp.int32, (count, width, width), 2)
    squares = jnp.sum(jnp.where(on_diagonal, shares[:, :width], 0.0))
    scaling = jnp.sqrt(norm_spread * squares / size + 1.0)
    gram = whole_matrix(shares * (1.0 / (scaling * scaling)))
    rows = lax.broadcasted_iota(jnp.int32, (size, width), 0)
    cols = lax.broadcasted_iota(jnp.int32, (size, width), 1) + place * width
    eye = jnp.where(rows == cols, 1.0, 0.0).astype(jnp.float32)

    def apply(gram, panel):
        first = mul(gram, panel)
        return (
            poly_linear * panel + poly_cubic * first + poly_quintic * mul(gram, first)
        )

    product = None
    for sweep in range(ITERS):
        if sweep == ITERS - 1:
            product = apply(gram, product)
            break
        panel = lax.dynamic_slice_in_dim(gram, place * width, width, 1)
        factor = poly_linear * eye + poly_cubic * panel + poly_quintic * mul(gram, panel)
        following = apply(gram, mul(gram, factor))
        coming = gather_shares(own_share(following, place, count))
        product = factor if product is None else apply(gram, product)
        coming, product = lax.optimization_barrier((coming, product))
        gram = whole_matrix(coming)
    rows_count = moment.shape[0] * lax.axis_size("fs")
    scaled = product * (math.sqrt(rows_count) / scaling)
    return mul(gathered, scaled, precision=lax.Precision.HIGH)


def per_device(grads, momentum):
    shares = lax.psum_scatter(grads[0], "rep", scatter_dimension=0, tiled=True)
    moment = momentum_decay * momentum + shares
    steps = [orthogonalize(moment[k]) for k in range(moment.shape[0])]
    return (moment, jnp.stack(steps))


def solution(mesh):
    placed = (P("rep", None, "fs", "tp"), P("rep", "fs", "tp"))
    return jax.shard_map(
        per_device,
        mesh=mesh,
        in_specs=placed,
        out_specs=(P("rep", "fs", "tp"), P("rep", "fs", "tp")),
        check_vma=False,
    )
```

profile of v0, /device:TPU:0, one launch (start us, length us, event | category | flops | bytes accessed | tf_op | source)
XLA Modules:
  0.0 1181.1 jit_solution(9694687099891742346)
XLA Ops:
  7.9 21.5 %reduce-scatter.3.cloned.1.call-done = f32[1,2048,512]{2,1,0:T(8,128)} async-done(((f32[2,2048,512]{2,1,0:T(8,128)}), f32[1,2048,512]{2,1,0:T(8,128)}) %reduce-scatter.3.cloned.1.call-update) | async-done | bytes 4194320 | tf_op jit(solution)/shard_map/reduce_scatter | solution.py:132
  29.4 6.5 multiply_add_fusion.6
  36.0 158.7 %all-gather.12.cloned.1.call-done = f32[1,2048,2048]{2,1,0:T(8,128)} async-done(((f32[1,2048,512]{2,1,0:T(8,128)}), f32[1,2048,2048]{2,1,0:T(8,128)}) %all-gather.12.cloned.1.call-update) | async-done | bytes 16777232 | tf_op jit(solution)/shard_map/all_gather | solution.py:90
  194.7 9.2 fusion.5
  203.9 9.3 fusion.8
  213.2 9.4 fusion.3
  224.4 52.4 %reduce-scatter.5.cloned.1.call-done = f32[320,512]{1,0:T(8,128)} async-done(((f32[1280,512]{1,0:T(8,128)}), f32[320,512]{1,0:T(8,128)}) %reduce-scatter.5.cloned.1.call-update) | async-done | bytes 655376 | tf_op jit(solution)/shard_map/reduce_scatter | solution.py:93
  276.8 55.7 %all-gather.10.cloned.1.call-done = f32[1280,512]{1,0:T(8,128)} async-done(((f32[320,512]{1,0:T(8,128)}), f32[1280,512]{1,0:T(8,128)}) %all-gather.10.cloned.1.call-update) | async-done | bytes 2621456 | tf_op jit(solution)/shard_map/all_gather | solution.py:96
  332.8 105.2 %all-gather.14.cloned.1.call-done = f32[5120,512]{1,0:T(8,128)} async-done(((f32[1280,512]{1,0:T(8,128)}), f32[5120,512]{1,0:T(8,128)}) %all-gather.14.cloned.1.call-update) | async-done | bytes 10485776 | tf_op jit(solution)/shard_map/all_gather | solution.py:40
  437.9 3.1 fusion.2
  441.7 5.9 broadcast_multiply_fusion
  459.5 7.9 dynamic_update_slice.144
  504.4 32.8 %multiply_add_fusion.3 = (f32[2048,512]{1,0:T(8,128)}, f32[2048,512]{1,0:T(8,128)S(1)}) fusion(f32[2048,2048]{1,0:T(8,128)} %fusion.56, s32[]{:T(128)S(6)} %select_n.50, s32[512]{0:T(512)S(1)} %iota_add_fusion), kind=kOutput, calls=%fused_computation.30 | convolution fusion | flops 25777143808 | bytes 33557504 | tf_op jit(solution)/shard_map/dot_general | solution.py:18
  537.2 34.0 %fusion.25 = f32[2048,512]{1,0:T(8,128)S(1)} fusion(f32[2048,2048]{1,0:T(8,128)} %fusion.56, f32[2048,512]{1,0:T(8,128)S(1)} %get-tuple-element.42, s32[]{:T(128)S(6)} %select_n.50, s32[512]{0:T(512)S(1)} %iota_add_fusion), kind=kOutput, calls=%fused_computation.31 | convolution fusion | flops 25777143808 | bytes 29362180 | tf_op jit(solution)/shard_map/dot_general | solution.py:18
  571.2 30.2 %fusion.93 = f32[2048,512]{1,0:T(8,128)S(1)} fusion(f32[2048,2048]{1,0:T(8,128)} %fusion.56, f32[2048,512]{1,0:T(8,128)S(1)} %fusion.25), kind=kOutput, calls=%fused_computation.184 | convolution fusion | flops 25769803776 | bytes 25165824 | tf_op jit(solution)/shard_map/dot_general | solution.py:18
  601.4 30.4 %multiply_add_fusion.2 = f32[2048,512]{1,0:T(8,128)S(1)} fusion(f32[2048,512]{1,0:T(8,128)S(1)} %fusion.93, f32[2048,512]{1,0:T(8,128)S(1)} %fusion.25, f32[2048,2048]{1,0:T(8,128)} %fusion.56), kind=kOutput, calls=%fused_computation.29 | convolution fusion | flops 25775046656 | bytes 29360128 | tf_op jit(solution)/shard_map/dot_general | solution.py:18
  637.2 105.0 %all-gather.16.cloned.1.call-done = f32[5120,512]{1,0:T(8,128)} async-done(((f32[1280,512]{1,0:T(8,128)}), f32[5120,512]{1,0:T(8,128)}) %all-gather.16.cloned.1.call-update) | async-done | bytes 10485776 | tf_op jit(solution)/shard_map/all_gather | solution.py:40
  742.2 4.3 slice_bitcast_fusion.16
  748.2 7.9 dynamic_update_slice.160
  802.5 33.0 %fusion.28 = f32[2048,512]{1,0:T(8,128)S(1)} fusion(f32[2048,2048]{1,0:T(8,128)} %bitcast_dynamic-update-slice_fusion.7, s32[]{:T(128)S(6)} %select_n.50), kind=kOutput, calls=%fused_computation.39 | convolution fusion | flops 25769803776 | bytes 25165828 | tf_op jit(solution)/shard_map/dot_general | solution.py:18
  835.5 31.3 %fusion.20 = f32[2048,512]{1,0:T(8,128)S(1)} fusion(f32[2048,2048]{1,0:T(8,128)S(1)} %copy-done.2, f32[2048,512]{1,0:T(8,128)S(1)} %fusion.28, s32[]{:T(128)S(6)} %select_n.50, s32[512]{0:T(512)S(1)} %iota_add_fusion), kind=kOutput, calls=%fused_computation.24 | convolution fusion | flops 25777143808 | bytes 29362180 | tf_op jit(solution)/shard_map/dot_general | solution.py:18
  866.8 28.4 %fusion.94 = f32[2048,512]{1,0:T(8,128)} fusion(f32[2048,2048]{1,0:T(8,128)S(1)} %copy-done.2, f32[2048,512]{1,0:T(8,128)S(1)} %fusion.20), kind=kOutput, calls=%fused_computation.185 | convolution fusion | flops 25769803776 | bytes 25165824 | tf_op jit(solution)/shard_map/dot_general | solution.py:18
  895.2 31.3 %multiply_add_fusion.1 = f32[2048,512]{1,0:T(8,128)S(1)} fusion(f32[2048,512]{1,0:T(8,128)} %fusion.94, f32[2048,512]{1,0:T(8,128)S(1)} %fusion.20, f32[2048,2048]{1,0:T(8,128)S(1)} %copy-done.2), kind=kOutput, calls=%fused_computation.23 | convolution fusion | flops 25775046656 | bytes 29360128 | tf_op jit(solution)/shard_map/dot_general | solution.py:18
  932.1 33.8 %fusion.95 = f32[2048,512]{1,0:T(8,128)S(1)} fusion(f32[2048,2048]{1,0:T(8,128)} %bitcast_dynamic-update-slice_fusion.7, f32[2048,512]{1,0:T(8,128)} %get-tuple-element.7), kind=kOutput, calls=%fused_computation.186 | convolution fusion | flops 25769803776 | bytes 25165824 | tf_op jit(solution)/shard_map/dot_general | solution.py:18
  966.0 31.5 %multiply_add_fusion = f32[2048,512]{1,0:T(8,128)} fusion(f32[2048,512]{1,0:T(8,128)S(1)} %fusion.95, f32[2048,512]{1,0:T(8,128)S(1)} %copy-done.9, f32[2048,2048]{1,0:T(8,128)} %bitcast_dynamic-update-slice_fusion.7), kind=kOutput, calls=%fused_computation.22 | convolution fusion | flops 25775046656 | bytes 29360128 | tf_op jit(solution)/shard_map/dot_general | solution.py:18
  997.4 39.7 %all-gather.18.cloned.1.call-done = f32[5120,512]{1,0:T(8,128)} async-done(((f32[1280,512]{1,0:T(8,128)}), f32[5120,512]{1,0:T(8,128)}) %all-gather.18.cloned.1.call-update) | async-done | bytes 10485776 | tf_op jit(solution)/shard_map/all_gather | solution.py:40
  1037.2 4.3 slice_bitcast_fusion.12
  1043.1 7.9 dynamic_update_slice.176
  1089.4 2.8 constant_dynamic-update-slice_fusion
  1098.0 30.7 %fusion.96 = f32[2048,512]{1,0:T(8,128)S(1)} fusion(f32[2048,2048]{1,0:T(8,128)} %bitcast_dynamic-update-slice_fusion, f32[2048,512]{1,0:T(8,128)S(1)} %copy-done.8), kind=kOutput, calls=%fused_computation.187 | convolution fusion | flops 25769803776 | bytes 25165824 | tf_op jit(solution)/shard_map/dot_general | solution.py:18
  1128.7 27.2 %fusion.97 = f32[2048,512]{1,0:T(8,128)S(1)} fusion(f32[2048,2048]{1,0:T(8,128)S(1)} %copy-done.1, f32[2048,512]{1,0:T(8,128)S(1)} %fusion.96), kind=kOutput, calls=%fused_computation.188 | convolution fusion | flops 25769803776 | bytes 25165824 | tf_op jit(solution)/shard_map/dot_general | solution.py:18
  1155.8 18.0 %fusion.33 = f32[1,2048,512]{2,1,0:T(8,128)} fusion(f32[2048,512]{1,0:T(8,128)S(1)} %fusion.97, f32[2048,512]{1,0:T(8,128)S(1)} %fusion.96, f32[2048,512]{1,0:T(8,128)S(1)} %copy-done.8, f32[1,2048,2048]{2,1,0:T(8,128)} %all-gather.12.cloned.1.call-done, f32[]{:T(128)S(6)} %div.11), kind=kOutput, calls=%fused_computation.44 | convolution fusion | flops 12891193344 | bytes 33554436 | tf_op jit(solution)/shard_map/dot_general | solution.py:18
  (119 shorter events, 156.5 us)
Async XLA Ops:
  7.2 22.2 %reduce-scatter.3.cloned.1.call-start = ((), (), s32[]{:S(2)}) async-start(), calls=%async_computation.2 | async-start | bytes 12582912 | tf_op jit(solution)/shard_map/reduce_scatter | solution.py:132
  7.9 186.8 %all-gather.12.cloned.1.call-start = ((), (), s32[]{:S(2)}) async-start(), calls=%async_computation.5 | async-start | bytes 20971520 | tf_op jit(solution)/shard_map/all_gather | solution.py:90
  35.9 240.8 %reduce-scatter.5.cloned.1.call-start = ((), (), s32[]{:S(2)}) async-start(), calls=%async_computation.3 | async-start | bytes 3276800 | tf_op jit(solution)/shard_map/reduce_scatter | solution.py:93
  224.3 108.2 %all-gather.10.cloned.1.call-start = ((), (), s32[]{:S(2)}) async-start(), calls=%async_computation.4 | async-start | bytes 3276800 | tf_op jit(solution)/shard_map/all_gather | solution.py:96
  276.8 161.1 %all-gather.14.cloned.1.call-start = ((), (), s32[]{:S(2)}) async-start(), calls=%async_computation.6 | async-start | bytes 13107200 | tf_op jit(solution)/shard_map/all_gather | solution.py:40
  332.5 409.7 %all-gather.16.cloned.1.call-start = ((), (), s32[]{:S(2)}) async-start(), calls=%async_computation.7 | async-start | bytes 13107200 | tf_op jit(solution)/shard_map/all_gather | solution.py:40
  447.6 5.2 copy-start
  459.5 7.9 copy-start.4
  459.5 9.0 copy-start.5
  471.9 21.9 %copy-start.3 = (f32[512,512]{0,1:T(8,128)S(1)}, f32[512,512]{0,1:T(8,128)}, u32[]{:S(2)}) copy-start(f32[512,512]{0,1:T(8,128)} %get-tuple-element.28) | copy-start | bytes 3145732
  631.8 2.0 copy-start.7
  637.1 400.1 %all-gather.18.cloned.1.call-start = ((), (), s32[]{:S(2)}) async-start(), calls=%async_computation.8 | async-start | bytes 13107200 | tf_op jit(solution)/shard_map/all_gather | solution.py:40
  802.5 33.0 %copy-start.2 = (f32[2048,2048]{1,0:T(8,128)S(1)}, f32[2048,2048]{1,0:T(8,128)}, u32[]{:S(2)}) copy-start(f32[2048,2048]{1,0:T(8,128)} %bitcast_dynamic-update-slice_fusion.7) | copy-start | bytes 50331652
  926.5 2.1 copy-start.6
  932.1 33.8 %copy-start.9 = (f32[2048,512]{1,0:T(8,128)S(1)}, f32[2048,512]{1,0:T(8,128)}, u32[]{:S(2)}) copy-start(f32[2048,512]{1,0:T(8,128)} %get-tuple-element.7) | copy-start | bytes 12582916
  1088.3 9.7 copy-start.8
  1098.0 30.7 %copy-start.1 = (f32[2048,2048]{1,0:T(8,128)S(1)}, f32[2048,2048]{1,0:T(8,128)}, u32[]{:S(2)}) copy-start(f32[2048,2048]{1,0:T(8,128)} %bitcast_dynamic-update-slice_fusion) | copy-start | bytes 50331652
Sparse Core Ops, SparseCore 0:
  10.3 19.1 reduce-scatter.2
  36.1 158.5 all-gather.11
  224.5 52.2 reduce-scatter.4
  278.2 54.2 all-gather.9
  334.2 103.6 all-gather.13
  637.2 104.9 all-gather.15
  932.2 104.9 all-gather.17
where the time goes:
time: 1190 us; the launch traced here: 1180 us
  waiting for transfers between devices  539 us (45%)
  matrix products  420 us (35%)
  local copies, waits for them, and re-layouts  171 us (14%)
  other arithmetic  35.2 us (3%)
  between operations  15.7 us (1%)
    dot_general x16, matrix products, mul(): lax.dot_general(a, b, (contract, ((), ())), precision=precision, preferre...  420 us
    all_gather x3, waiting for transfers between devices, gather_shares(): return lax.all_gather(share, 'tp', axis=0, tiled=False)  250 us
    all_gather x1, waiting for transfers between devices, orthogonalize(): gathered = lax.all_gather(moment, 'tp', axis=1, tiled=True)  159 us
    dynamic_update_slice x42, local copies, waits for them, and re-layouts, whole_matrix(): lax.dynamic_update_slice(matrix, block(row, col), (row * width, col * wid...  109 us
    all_gather x1, waiting for transfers between devices, orthogonalize(): share = lax.all_gather(share, 'fs', axis=0, tiled=True)  55.7 us
    reduce_scatter x1, waiting for transfers between devices, orthogonalize(): lax.psum_scatter(gram_share(gathered, place, count), 'fs', scatter_dimens...  52.4 us
    transpose x21, local copies, waits for them, and re-layouts, block(): return block(col, row).T  50.3 us
  transfers between devices with their start and end apart: 7, of which 7 were waited for; matrix products, arithmetic and copies ran while one was open for 6% of the time, Pallas kernels for 0%

commit v1 on v0

v1 whole, which is shorter than its diff:
```python
import functools
import math

import jax
import jax.numpy as jnp
from jax import lax
from jax.experimental import pallas as pl
from jax.experimental.pallas import tpu as pltpu
from jax.sharding import PartitionSpec as P

ITERS = 3

momentum_decay = 0.95
norm_spread = 2.56
poly_linear = 3.4445
poly_cubic = -4.775
poly_quintic = 2.0315

MESH = pl.DeviceIdType.MESH
VMEM_BYTES = 63 * 1024 * 1024
SLOTS = 5


def split(value):
    high = value.astype(jnp.bfloat16)
    low = (value - high.astype(jnp.float32)).astype(jnp.bfloat16)
    return high, low


def dot3(a_high, a_low, b_high, b_low, contract=((1,), (0,))):
    def one(a, b):
        return lax.dot_general(
            a, b, (contract, ((), ())), preferred_element_type=jnp.float32
        )

    return one(a_high, b_high) + one(a_high, b_low) + one(a_low, b_high)


def bits(place):
    y = place // 2
    return place - 2 * y, y


def partner(place, s):
    x, y = bits(place)
    return (place, place + 1 - 2 * x, place + 2 - 4 * y, 3 - place)[s]


def block_row(place, chunk, slot):
    x, y = bits(place)
    if slot == 0:
        return 2 * place + chunk
    if slot == 1:
        return 2 * place + 1 - chunk
    s = slot - 1
    flip = x if s == 1 else y
    return 2 * partner(place, s) + chunk + flip - 2 * chunk * flip


def gram_kernel(x_ref, out_ref, high_ref, low_ref):
    place = lax.axis_index("tp")
    half = out_ref.shape[-1]

    @pl.when(pl.program_id(0) == 0)
    def _():
        out_ref[...] = jnp.zeros_like(out_ref)

    for q in range(x_ref.shape[0]):
        for side in range(2):
            high, low = split(x_ref[q, :, side * half : (side + 1) * half])
            high_ref[2 * q + side] = high
            low_ref[2 * q + side] = low
    for chunk in range(2):
        own = 2 * place + chunk
        for slot in range(SLOTS):
            if slot == 1 and chunk == 1:
                continue
            row = block_row(place, chunk, slot)
            out_ref[chunk, slot] += dot3(
                high_ref[row], low_ref[row], high_ref[own], low_ref[own], ((0,), (0,))
            )


def gram_share(gathered):
    count, rows, width = gathered.shape
    half = width // 2
    tile = min(rows, 512)
    return pl.pallas_call(
        gram_kernel,
        grid=(rows // tile,),
        in_specs=[pl.BlockSpec((count, tile, width), lambda i: (0, i, 0))],
        out_specs=pl.BlockSpec((2, SLOTS, half, half), lambda i: (0, 0, 0, 0)),
        out_shape=jax.ShapeDtypeStruct((2, SLOTS, half, half), jnp.float32),
        scratch_shapes=[
            pltpu.VMEM((2 * count, tile, half), jnp.bfloat16),
            pltpu.VMEM((2 * count, tile, half), jnp.bfloat16),
        ],
        compiler_params=pltpu.CompilerParams(
            vmem_limit_bytes=VMEM_BYTES, dimension_semantics=("arbitrary",)
        ),
        cost_estimate=pl.CostEstimate(
            flops=2 * 3 * 9 * rows * half * half,
            bytes_accessed=4 * rows * count * width,
            transcendentals=0,
        ),
    )(gathered)


def iterate_kernel(
    rows_count,
    share_ref,
    out_high,
    out_low,
    held,
    gram_high,
    gram_low,
    op_high,
    op_low,
    first,
    second,
    product,
    wide_high,
    wide_low,
    send_sem,
    recv_sem,
    free_sem,
):
    size = gram_high.shape[0]
    half = held.shape[-1]
    place = lax.axis_index("tp")
    neighbours = (None, partner(place, 1), partner(place, 2))
    tile = 2 * half
    tiles = size // tile

    def panel_cols(chunk):
        return pl.ds(pl.multiple_of((2 * place + chunk) * half, half), half)

    def rows_of(block, count=1):
        return pl.ds(pl.multiple_of(block * half, half), half * count)

    def eye(at):
        shape = (tile, half)
        rows = lax.broadcasted_iota(jnp.int32, shape, 0) + at * tile
        return lambda col: rows == lax.broadcasted_iota(jnp.int32, shape, 1) + col

    def copy(via, chunk, slot):
        if via == 0:
            source, target, to = held.at[0, chunk, slot], held.at[1, chunk, slot], 1
        elif via == 1:
            source, target, to = held.at[0, chunk, slot], held.at[2, chunk, slot], 2
        elif over_y(chunk, slot):
            source, target, to = held.at[1, chunk, slot], held.at[3, chunk, slot], 2
        else:
            source, target, to = held.at[2, chunk, slot], held.at[3, chunk, slot], 1
        return pltpu.make_async_remote_copy(
            src_ref=source,
            dst_ref=target,
            send_sem=send_sem.at[via, chunk, slot],
            recv_sem=recv_sem.at[via, chunk, slot],
            device_id={"tp": neighbours[to]},
            device_id_type=MESH,
        )

    def over_y(chunk, slot):
        order = [k for k in range(SLOTS) if not (chunk == 1 and k == 1)]
        place_in = order.index(slot)
        return place_in % 2 == chunk

    def slots(chunk):
        return [k for k in range(SLOTS) if not (chunk == 1 and k == 1)]

    def send(chunk, slot):
        copy(0, chunk, slot).start()
        copy(1, chunk, slot).start()

    def relay(chunk):
        for slot in slots(chunk):
            copy(0, chunk, slot).wait_recv()
            copy(1, chunk, slot).wait_recv()
            copy(2, chunk, slot).start()

    def assemble(s, chunk):
        q = partner(place, s)
        col = 2 * q + chunk
        for slot in slots(chunk):
            row = block_row(q, chunk, slot)
            value = held[s, chunk, slot]
            high, low = split(value)
            gram_high[rows_of(row), rows_of(col)] = high
            gram_low[rows_of(row), rows_of(col)] = low
            if slot > 0:
                high, low = split(value.T)
                gram_high[rows_of(col), rows_of(row)] = high
                gram_low[rows_of(col), rows_of(row)] = low

    def exchange(between):
        relay(0)
        between()
        assemble(0, 0)
        assemble(0, 1)
        for s in (1, 2):
            assemble(s, 0)
        relay(1)
        for s in (1, 2):
            assemble(s, 1)
        for chunk in range(2):
            for slot in slots(chunk):
                copy(2, chunk, slot).wait_recv()
            assemble(3, chunk)
        for via in range(3):
            for chunk in range(2):
                for slot in slots(chunk):
                    copy(via, chunk, slot).wait_send()

    def times_gram(at, count, high, low):
        rows = rows_of(at, count)
        return dot3(gram_high[rows, :], gram_low[rows, :], high, low)

    def sweep_factor(chunk, scale, also):
        def body(at, _):
            cols = panel_cols(chunk)
            rows = rows_of(2 * at, 2)
            own = gram_high[rows, cols].astype(jnp.float32) + gram_low[rows, cols].astype(
                jnp.float32
            )
            double = times_gram(2 * at, 2, gram_high[:, cols], gram_low[:, cols])
            linear = jnp.where(eye(at)((2 * place + chunk) * half), poly_linear, 0.0)
            factor = (
                linear + (poly_cubic * scale) * own + (poly_quintic * scale * scale) * double
            )
            high, low = split(factor)
            op_high[0, rows, :] = high
            op_low[0, rows, :] = low
            also(rows, factor)
            return 0

        lax.fori_loop(0, tiles, body, 0)

    def times(source, target, keep, scale):
        def body(at, _):
            rows = rows_of(2 * at, 2)
            value = scale * times_gram(2 * at, 2, op_high[source], op_low[source])
            keep[rows, :] = value
            high, low = split(value)
            op_high[target, rows, :] = high
            op_low[target, rows, :] = low
            return 0

        lax.fori_loop(0, tiles, body, 0)

    def following(chunk, scale):
        behind = None
        for slot in slots(chunk):
            row = block_row(place, chunk, slot)
            rows = rows_of(row)
            value = scale * times_gram(row, 1, op_high[0], op_low[0])
            held[0, chunk, slot] = (
                poly_linear * first[rows, :]
                + poly_cubic * second[rows, :]
                + poly_quintic * value
            )
            if behind is not None:
                send(chunk, behind)
            behind = slot
        send(chunk, behind)

    def apply(scale, finish):
        def body(at, _):
            rows = rows_of(2 * at, 2)
            part = times_gram(2 * at, 2, wide_high[0], wide_low[0])
            value = scale * part
            product[rows, :] = poly_linear * product[rows, :] + poly_cubic * value
            high, low = split(value)
            wide_high[1, rows, :] = high
            wide_low[1, rows, :] = low
            return 0

        lax.fori_loop(0, tiles, body, 0)

        def body2(at, _):
            rows = rows_of(2 * at, 2)
            part = scale * times_gram(2 * at, 2, wide_high[1], wide_low[1])
            finish(rows, product[rows, :] + poly_quintic * part)
            return 0

        lax.fori_loop(0, tiles, body2, 0)

    def keep_product(rows, value):
        product[rows, :] = value
        high, low = split(value)
        wide_high[0, rows, :] = high
        wide_low[0, rows, :] = low

    barrier = pltpu.get_barrier_semaphore()
    for to in (1, 2):
        pl.semaphore_signal(
            barrier, inc=1, device_id={"tp": neighbours[to]}, device_id_type=MESH
        )
    held[0] = share_ref[...]
    pl.semaphore_wait(barrier, 2)
    for chunk in range(2):
        for slot in slots(chunk):
            send(chunk, slot)
    exchange(lambda: None)

    on_diagonal = lax.broadcasted_iota(
        jnp.int32, (half, half), 0
    ) == lax.broadcasted_iota(jnp.int32, (half, half), 1)
    squares = jnp.zeros((1, 1), jnp.float32)
    for s in range(4):
        for chunk in range(2):
            picked = jnp.where(on_diagonal, held[s, chunk, 0], 0.0)
            squares += jnp.sum(
                jnp.sum(picked, axis=0, keepdims=True), axis=1, keepdims=True
            )
    scaling = jnp.sqrt(squares * (norm_spread / size) + 1.0)
    scale = 1.0 / (scaling * scaling)

    for sweep in range(ITERS):
        if sweep == ITERS - 1:
            last = math.sqrt(rows_count) / scaling

            def finish(rows, value):
                high, low = split(value * last)
                out_high[rows, :] = high
                out_low[rows, :] = low

            apply(scale, finish)
            break
        for to in (1, 2):
            pl.semaphore_signal(
                free_sem, inc=1, device_id={"tp": neighbours[to]}, device_id_type=MESH
            )
        for chunk in range(2):

            def also(rows, factor):
                if sweep == 0:
                    cols = slice(chunk * half, (chunk + 1) * half)
                    product[rows, cols] = factor
                    high, low = split(factor)
                    wide_high[0, rows, cols] = high
                    wide_low[0, rows, cols] = low

            sweep_factor(chunk, scale, also)
            times(0, 1, first, scale)
            times(1, 0, second, scale)
            if chunk == 0:
                pl.semaphore_wait(free_sem, 2)
            following(chunk, scale)
        if sweep == 0:
            exchange(lambda: None)
        else:
            exchange(lambda: apply(scale, keep_product))
        scale = jnp.ones((1, 1), jnp.float32)


def polynomial(share, rows_count):
    half = share.shape[-1]
    size = 8 * half
    wide = jax.ShapeDtypeStruct((size, 2 * half), jnp.bfloat16)
    return pl.pallas_call(
        functools.partial(iterate_kernel, rows_count),
        out_shape=(wide, wide),
        in_specs=[pl.BlockSpec(memory_space=pltpu.VMEM)],
        out_specs=(pl.BlockSpec(memory_space=pltpu.VMEM),) * 2,
        scratch_shapes=[
            pltpu.VMEM((4, 2, SLOTS, half, half), jnp.float32),
            pltpu.VMEM((size, size), jnp.bfloat16),
            pltpu.VMEM((size, size), jnp.bfloat16),
            pltpu.VMEM((2, size, half), jnp.bfloat16),
            pltpu.VMEM((2, size, half), jnp.bfloat16),
            pltpu.VMEM((size, half), jnp.float32),
            pltpu.VMEM((size, half), jnp.float32),
            pltpu.VMEM((size, 2 * half), jnp.float32),
            pltpu.VMEM((2, size, 2 * half), jnp.bfloat16),
            pltpu.VMEM((2, size, 2 * half), jnp.bfloat16),
            pltpu.SemaphoreType.DMA((3, 2, SLOTS)),
            pltpu.SemaphoreType.DMA((3, 2, SLOTS)),
            pltpu.SemaphoreType.REGULAR,
        ],
        compiler_params=pltpu.CompilerParams(
            collective_id=0, has_side_effects=True, vmem_limit_bytes=VMEM_BYTES
        ),
        cost_estimate=pl.CostEstimate(
            flops=2 * 3 * 12 * size * size * 2 * half,
            bytes_accessed=8 * size * 2 * half,
            transcendentals=0,
        ),
    )(share)


def step_kernel(x_ref, high_ref, low_ref, out_ref):
    width = x_ref.shape[-1]
    total = None
    for q in range(x_ref.shape[0]):
        x_high, x_low = split(x_ref[q])
        rows = slice(q * width, (q + 1) * width)
        part = dot3(x_high, x_low, high_ref[rows, :], low_ref[rows, :])
        total = part if total is None else total + part
    out_ref[...] = total


def step_of(gathered, high, low):
    count, rows, width = gathered.shape
    tile = min(rows, 256)
    whole = pl.BlockSpec((count * width, width), lambda i: (0, 0))
    return pl.pallas_call(
        step_kernel,
        grid=(rows // tile,),
        in_specs=[
            pl.BlockSpec((count, tile, width), lambda i: (0, i, 0)),
            whole,
            whole,
        ],
        out_specs=pl.BlockSpec((tile, width), lambda i: (i, 0)),
        out_shape=jax.ShapeDtypeStruct((rows, width), jnp.float32),
        compiler_params=pltpu.CompilerParams(
            vmem_limit_bytes=VMEM_BYTES, dimension_semantics=("arbitrary",)
        ),
        cost_estimate=pl.CostEstimate(
            flops=2 * 3 * rows * count * width * width,
            bytes_accessed=4 * rows * (count + 1) * width,
            transcendentals=0,
        ),
    )(gathered, high, low)


def orthogonalize(moment):
    rows_count = moment.shape[0] * lax.axis_size("fs")
    gathered = lax.all_gather(moment, "tp", axis=0, tiled=False)
    share = gram_share(gathered)
    shape = share.shape
    share = share.reshape(-1, shape[-1])
    share = lax.psum_scatter(share, "fs", scatter_dimension=0, tiled=True)
    share = lax.all_gather(share, "fs", axis=0, tiled=True).reshape(shape)
    high, low = polynomial(share, rows_count)
    return step_of(gathered, high, low)


def per_device(grads, momentum):
    shares = lax.psum_scatter(grads[0], "rep", scatter_dimension=0, tiled=True)
    moment = momentum_decay * momentum + shares
    steps = [orthogonalize(moment[k]) for k in range(moment.shape[0])]
    return (moment, jnp.stack(steps))


def solution(mesh):
    placed = (P("rep", None, "fs", "tp"), P("rep", "fs", "tp"))
    return jax.shard_map(
        per_device,
        mesh=mesh,
        in_specs=placed,
        out_specs=(P("rep", "fs", "tp"), P("rep", "fs", "tp")),
        check_vma=False,
    )
```

time: 1190 us -> 675 us (0.57)
  matrix products: 420 us -> 0 us
  Pallas kernels: 0 us -> 359 us
  waiting for transfers between devices: 539 us -> 289 us
  local copies, waits for them, and re-layouts: 171 us -> 0 us
  other arithmetic: 35.2 us -> 6.51 us
    dot_general x16 -> x0, matrix products: 420 us -> none  [mul(): lax.dot_general(a, b, (contract, ((), ())), precision=precision, preferre...]
    pallas_call x0 -> x3, Pallas kernels: none -> 359 us  [the longest x1 325 us: polynomial(): pl.pallas_call(functools.partial(iterate_kernel, rows_count), out_shape=(...]
    all_gather x5 -> x2, waiting for transfers between devices: 464 us -> 214 us  [the longest x1 159 us: orthogonalize(): gathered = lax.all_gather(moment, 'tp', axis=0, tiled=False)]
    dynamic_update_slice x42 -> x0, local copies, waits for them, and re-layouts: 109 us -> none  [whole_matrix(): lax.dynamic_update_slice(matrix, block(row, col), (row * width, col * wid...]
    transpose x21 -> x0, local copies, waits for them, and re-layouts: 50.3 us -> none  [block(): return block(col, row).T]
  transfers between devices with their start and end apart: 7 -> 4, of which waited for: 7 -> 4; matrix products, arithmetic and copies ran while one was open for 6% -> 0% of each run, Pallas kernels for 0% -> 0%
where the time goes in v1:
time: 675 us; the launch traced here: 669 us
  Pallas kernels  359 us (53%)
  waiting for transfers between devices  289 us (43%)
  between operations  14.2 us (2%)
    pallas_call x1, Pallas kernels, polynomial(): pl.pallas_call(functools.partial(iterate_kernel, rows_count), out_shape=(...  325 us
    all_gather x1, waiting for transfers between devices, orthogonalize(): gathered = lax.all_gather(moment, 'tp', axis=0, tiled=False)  159 us
    all_gather x1, waiting for transfers between devices, orthogonalize(): share = lax.all_gather(share, 'fs', axis=0, tiled=True).reshape(shape)  55.7 us
    reduce_scatter x1, waiting for transfers between devices, orthogonalize(): share = lax.psum_scatter(share, 'fs', scatter_dimension=0, tiled=True)  52.4 us
    reduce_scatter x1, waiting for transfers between devices, per_device(): shares = lax.psum_scatter(grads[0], 'rep', scatter_dimension=0, tiled=True)  21.5 us
    pallas_call x1, Pallas kernels, step_of(): pl.pallas_call(step_kernel, grid=(rows // tile,), in_specs=[pl.BlockSpec(...  18.1 us
    pallas_call x1, Pallas kernels, gram_share(): pl.pallas_call(gram_kernel, grid=(rows // tile,), in_specs=[pl.BlockSpec(...  15.7 us
  transfers between devices with their start and end apart: 4, of which 4 were waited for; matrix products, arithmetic and copies ran while one was open for 0% of the time, Pallas kernels for 0%

profile of v1, /device:TPU:0, one launch (start us, length us, event | category | flops | bytes accessed | tf_op | source)
XLA Modules:
  0.0 668.8 jit_solution(9885448247804779005)
XLA Ops:
  7.2 0.0 reduce-scatter.3.cloned.1.call-start
  7.2 0.7 reduce-scatter.3.cloned.1.call-update
  7.9 0.0 all-gather.3.cloned.1.call-start
  7.9 21.5 %reduce-scatter.3.cloned.1.call-done = f32[1,2048,512]{2,1,0:T(8,128)} async-done(((f32[2,2048,512]{2,1,0:T(8,128)}), f32[1,2048,512]{2,1,0:T(8,128)}) %reduce-scatter.3.cloned.1.call-update) | async-done | bytes 4194320 | tf_op jit(solution)/shard_map/reduce_scatter | solution.py:441
  29.4 6.5 multiply_add_fusion
  35.9 0.0 all-gather.3.cloned.1.call-update
  35.9 0.0 reduce-scatter.5.cloned.1.call-start
  36.0 158.7 %all-gather.3.cloned.1.call-done.x_ref = f32[4,2048,512]{2,1,0:T(8,128)} async-done(((f32[1,2048,512]{2,1,0:T(8,128)}), f32[4,2048,512]{2,1,0:T(8,128)}) %all-gather.3.cloned.1.call-update) | async-done | bytes 16777232 | tf_op jit(solution)/shard_map/all_gather | solution.py:430
  194.7 15.7 %shard_map.41 = f32[2,5,256,256]{3,2,1,0:T(8,128)} custom-call(f32[4,2048,512]{2,1,0:T(8,128)} %all-gather.3.cloned.1.call-done.x_ref), custom_call_target="tpu_custom_call" | custom-call | flops 7247757312 | bytes 16777216 | tf_op jit(solution)/shard_map/pallas_call | solution.py:88
  210.4 0.0 reduce-scatter.5.cloned.1.call-update
  210.4 0.0 all-gather.5.cloned.1.call-start
  210.5 52.4 %reduce-scatter.5.cloned.1.call-done = f32[640,256]{1,0:T(8,128)} async-done(((f32[2560,256]{1,0:T(8,128)}), f32[640,256]{1,0:T(8,128)}) %reduce-scatter.5.cloned.1.call-update) | async-done | bytes 655376 | tf_op jit(solution)/shard_map/reduce_scatter | solution.py:434
  262.8 0.0 all-gather.5.cloned.1.call-update
  262.9 55.7 %all-gather.5.cloned.1.call-done = f32[2560,256]{1,0:T(8,128)} async-done(((f32[640,256]{1,0:T(8,128)}), f32[2560,256]{1,0:T(8,128)}) %all-gather.5.cloned.1.call-update) | async-done | bytes 2621456 | tf_op jit(solution)/shard_map/all_gather | solution.py:435
  318.6 325.2 %shard_map.42 = (bf16[2048,512]{1,0:T(8,128)(2,1)}, bf16[2048,512]{1,0:T(8,128)(2,1)}) custom-call(f32[2,5,256,256]{3,2,1,0:T(8,128)} %bitcast.6), custom_call_target="tpu_custom_call" | custom-call | flops 154618822656 | bytes 8388608 | tf_op jit(solution)/shard_map/pallas_call | solution.py:361
  643.8 18.1 %shard_map.43 = f32[2048,512]{1,0:T(8,128)} custom-call(f32[4,2048,512]{2,1,0:T(8,128)} %all-gather.3.cloned.1.call-done.x_ref, bf16[2048,512]{1,0:T(8,128)(2,1)} %get-tuple-element.4.high_ref, bf16[2048,512]{1,0:T(8,128)(2,1)} %get-tuple-element.5.low_ref), custom_call_target="tpu_custom_call" | custom-call | flops 12884901888 | bytes 20971520 | tf_op jit(solution)/shard_map/pallas_call | solution.py:407
Async XLA Ops:
  7.2 22.2 %reduce-scatter.3.cloned.1.call-start = ((), (), s32[]{:S(2)}) async-start(), calls=%async_computation.2 | async-start | bytes 12582912 | tf_op jit(solution)/shard_map/reduce_scatter | solution.py:441
  7.9 186.8 %all-gather.3.cloned.1.call-start = ((), (), s32[]{:S(2)}) async-start(), calls=%async_computation.3 | async-start | bytes 20971520 | tf_op jit(solution)/shard_map/all_gather | solution.py:430
  35.9 226.9 %reduce-scatter.5.cloned.1.call-start = ((), (), s32[]{:S(2)}) async-start(), calls=%async_computation.4 | async-start | bytes 3276800 | tf_op jit(solution)/shard_map/reduce_scatter | solution.py:434
  210.4 108.2 %all-gather.5.cloned.1.call-start = ((), (), s32[]{:S(2)}) async-start(), calls=%async_computation.5 | async-start | bytes 3276800 | tf_op jit(solution)/shard_map/all_gather | solution.py:435
Sparse Core Ops, SparseCore 0:
  10.3 19.1 reduce-scatter.2
  36.1 158.5 all-gather.2
  210.5 52.2 reduce-scatter.4
  264.3 54.2 all-gather.4

commit v2 on v1

--- a/solution.py
+++ b/solution.py
@@ -19,6 +19,7 @@
 MESH = pl.DeviceIdType.MESH
 VMEM_BYTES = 63 * 1024 * 1024
 SLOTS = 5
+PIECES = 4
 
 
 def split(value):
@@ -57,53 +58,325 @@
     return 2 * partner(place, s) + chunk + flip - 2 * chunk * flip
 
 
-def gram_kernel(x_ref, out_ref, high_ref, low_ref):
+def front_kernel(
+    peers,
+    grads_ref,
+    momentum_ref,
+    moment_out,
+    share_out,
+    high_out,
+    low_out,
+    grads_own,
+    grads_other,
+    own,
+    land,
+    x_high,
+    x_low,
+    part,
+    parts,
+    share,
+    local_sem,
+    out_sem,
+    rep_send,
+    rep_recv,
+    x_send,
+    x_recv,
+    sum_send,
+    sum_recv,
+    all_send,
+    all_recv,
+):
     place = lax.axis_index("tp")
-    half = out_ref.shape[-1]
-
-    @pl.when(pl.program_id(0) == 0)
-    def _():
-        out_ref[...] = jnp.zeros_like(out_ref)
-
-    for q in range(x_ref.shape[0]):
-        for side in range(2):
-            high, low = split(x_ref[q, :, side * half : (side + 1) * half])
-            high_ref[2 * q + side] = high
-            low_ref[2 * q + side] = low
-    for chunk in range(2):
-        own = 2 * place + chunk
-        for slot in range(SLOTS):
-            if slot == 1 and chunk == 1:
-                continue
-            row = block_row(place, chunk, slot)
-            out_ref[chunk, slot] += dot3(
-                high_ref[row], low_ref[row], high_ref[own], low_ref[own], ((0,), (0,))
-            )
-
-
-def gram_share(gathered):
-    count, rows, width = gathered.shape
+    layer = lax.axis_index("fs")
+    core = lax.axis_index("rep")
+    x, y = bits(place)
+    neighbours = (None, partner(place, 1), partner(place, 2))
+    rows, half = own.shape[1:]
+    step = rows // PIECES
+    slab = half // peers
+
+    barrier = pltpu.get_barrier_semaphore()
+    pl.semaphore_signal(
+        barrier, inc=1, device_id={"rep": 1 - core}, device_id_type=MESH
+    )
+    for to in (1, 2):
+        pl.semaphore_signal(
+            barrier, inc=1, device_id={"tp": neighbours[to]}, device_id_type=MESH
+        )
+
+    def greet(d, _):
+        pl.semaphore_signal(
+            barrier,
+            inc=1,
+            device_id={"fs": lax.rem(layer + d, peers)},
+            device_id_type=MESH,
+        )
+        return 0
+
+    lax.fori_loop(1, peers, greet, 0)
+
+    def at(piece):
+        return pl.ds(piece * step, step)
+
+    def fetch(piece):
+        return pltpu.make_async_copy(
+            grads_ref.at[0, core, at(piece)], grads_own.at[at(piece)], local_sem.at[piece]
+        )
+
+    def give(piece):
+        return pltpu.make_async_remote_copy(
+            src_ref=grads_ref.at[0, 1 - core, at(piece)],
+            dst_ref=grads_other.at[at(piece)],
+            send_sem=rep_send.at[piece],
+            recv_sem=rep_recv.at[piece],
+            device_id={"rep": 1 - core},
+            device_id_type=MESH,
+        )
+
+    def copy(via, side, piece):
+        if via < 2:
+            source, to, lands = own, via + 1, via
+            source = own.at[side, at(piece)]
+        else:
+            source = land.at[piece % 2, side, at(piece)]
+            to, lands = 2 - piece % 2, 2
+        return pltpu.make_async_remote_copy(
+            src_ref=source,
+            dst_ref=land.at[lands, side, at(piece)],
+            send_sem=x_send.at[via, side, piece],
+            recv_sem=x_recv.at[via, side, piece],
+            device_id={"tp": neighbours[to]},
+            device_id_type=MESH,
+        )
+
+    def send(side, piece):
+        copy(0, side, piece).start()
+        copy(1, side, piece).start()
+
+    def relay(side, piece):
+        copy(0, side, piece).wait_recv()
+        copy(1, side, piece).wait_recv()
+        copy(2, side, piece).start()
+
+    tile = min(step, 128)
+
+    def keep(s, side, rows_at, value):
+        high, low = split(value)
+        x_high[s, side, rows_at] = high
+        x_low[s, side, rows_at] = low
+
+    def divide(s, side):
+        def body(k, _):
+            rows_at = pl.ds(pl.multiple_of(k * tile, tile), tile)
+            keep(s, side, rows_at, land[s - 1, side, rows_at])
+            return 0
+
+        lax.fori_loop(0, rows // tile, body, 0)
+
+    def out_copies(s, side):
+        return (
+            pltpu.make_async_copy(
+                x_high.at[s, side], high_out.at[s, side], out_sem.at[0, s, side]
+            ),
+            pltpu.make_async_copy(
+                x_low.at[s, side], low_out.at[s, side], out_sem.at[1, s, side]
+            ),
+        )
+
+    def moment_copy(side):
+        return pltpu.make_async_copy(
+            own.at[side],
+            moment_out.at[0, :, pl.ds(side * half, half)],
+            out_sem.at[2, 0, side],
+        )
+
+    def chunk_of(s, side):
+        flip = x if s == 1 else y
+        return side + flip - 2 * side * flip
+
+    keys = [(0, 0, 0), (0, 1, 1), (0, 0, 1)]
+    homes = [(0, 0), (1, 0), (0, 1)]
+    for side in range(2):
+        for s in (1, 2, 3):
+            keys.append((s, side, None))
+            homes.append((chunk_of(s, side), 1 + s))
+
+    def block(key):
+        s, side, chunk = keys[key]
+        if s == 0:
+            lhs, rhs = (0, chunk), (0, side)
+        else:
+            lhs, rhs = (s, side), (0, chunk_of(s, side))
+        part[key] = dot3(
+            x_high[lhs], x_low[lhs], x_high[rhs], x_low[rhs], ((0,), (0,))
+        )
+
+        def scatter(d, _):
+            target = lax.rem(layer + d, peers)
+            pltpu.make_async_remote_copy(
+                src_ref=part.at[key, pl.ds(pl.multiple_of(target * slab, slab), slab)],
+                dst_ref=parts.at[key, d - 1],
+                send_sem=sum_send.at[key],
+                recv_sem=sum_recv.at[key],
+                device_id={"fs": target},
+                device_id_type=MESH,
+            ).start()
+            return 0
+
+        lax.fori_loop(1, peers, scatter, 0)
+
+    def all_of(key, send_sem, recv_sem):
+        return pltpu.make_async_remote_copy(
+            src_ref=parts.at[key],
+            dst_ref=parts.at[key],
+            send_sem=send_sem.at[key],
+            recv_sem=recv_sem.at[key],
+            device_id={"fs": lax.rem(layer + 1, peers)},
+            device_id_type=MESH,
+        )
+
+    def total(key):
+        all_of(key, sum_send, sum_recv).wait_recv()
+        mine = pl.ds(pl.multiple_of(layer * slab, slab), slab)
+        value = part[key, mine]
+        for d in range(peers - 1):
+            value = value + parts[key, d]
+        chunk, slot = homes[key]
+        share[chunk, slot, mine] = value
+
+        def spread(d, _):
+            pltpu.make_async_remote_copy(
+                src_ref=share.at[chunk, slot, mine],
+                dst_ref=share.at[chunk, slot, mine],
+                send_sem=all_send.at[key],
+                recv_sem=all_recv.at[key],
+                device_id={"fs": lax.rem(layer + d, peers)},
+                device_id_type=MESH,
+            ).start()
+            return 0
+
+        lax.fori_loop(1, peers, spread, 0)
+
+    for piece in range(PIECES):
+        fetch(piece).start()
+    pl.semaphore_wait(barrier, 3 + peers - 1)
+    for piece in range(PIECES):
+        give(piece).start()
+    for piece in range(PIECES):
+        fetch(piece).wait()
+        give(piece).wait_recv()
+
+        def add(k, _):
+            rows_at = pl.ds(pl.multiple_of(piece * step + k * tile, tile), tile)
+            for side in range(2):
+                cols = slice(side * half, (side + 1) * half)
+                value = momentum_decay * momentum_ref[0, rows_at, cols] + (
+                    grads_own[rows_at, cols] + grads_other[rows_at, cols]
+                )
+                own[side, rows_at] = value
+                keep(0, side, rows_at, value)
+            return 0
+
+        lax.fori_loop(0, step // tile, add, 0)
+        if piece > 0:
+            send(0, piece - 1)
+    send(0, PIECES - 1)
+    send(1, 0)
+    for side in range(2):
+        moment_copy(side).start()
+        for each in out_copies(0, side):
+            each.start()
+    share[1, 1] = jnp.zeros((half, half), jnp.float32)
+    for key in range(3):
+        block(key)
+    for side in range(2):
+        for piece in range(PIECES):
+            relay(side, piece)
+            if side == 0 and piece + 1 < PIECES:
+                send(1, piece + 1)
+        for s in (1, 2):
+            divide(s, side)
+            for each in out_copies(s, side):
+                each.start()
+            block(3 + 3 * side + s - 1)
+        for key in (range(3) if side == 0 else (5,)):
+            total(key)
+        for piece in range(PIECES):
+            copy(2, side, piece).wait_recv()
+        divide(3, side)
+        for each in out_copies(3, side):
+            each.start()
+        block(5 + 3 * side)
+        for s in (1, 2):
+            total(3 + 3 * side + s - 1)
+    total(8)
+    for side in range(2):
+        moment_copy(side).wait()
+        for s in range(4):
+            for each in out_copies(s, side):
+                each.wait()
+        for piece in range(PIECES):
+            for via in range(3):
+                copy(via, side, piece).wait_send()
+    for piece in range(PIECES):
+        give(piece).wait_send()
+    for key in range(9):
+        all_of(key, sum_send, sum_recv).wait_send()
+        all_of(key, all_send, all_recv).wait_send()
+    for key in range(9):
+        all_of(key, all_send, all_recv).wait_recv()
+    share_out[...] = share[...]
+
+
+def front(grads, momentum):
+    peers = lax.axis_size("fs")
+    _, rows, width = momentum.shape
     half = width // 2
-    tile = min(rows, 512)
+    slab = half // peers
+    parts = jax.ShapeDtypeStruct((4, 2, rows, half), jnp.bfloat16)
+    anywhere = pl.BlockSpec(memory_space=pl.ANY)
+    vmem = pl.BlockSpec(memory_space=pltpu.VMEM)
+    semaphores = pltpu.SemaphoreType.DMA
     return pl.pallas_call(
-        gram_kernel,
-        grid=(rows // tile,),
-        in_specs=[pl.BlockSpec((count, tile, width), lambda i: (0, i, 0))],
-        out_specs=pl.BlockSpec((2, SLOTS, half, half), lambda i: (0, 0, 0, 0)),
-        out_shape=jax.ShapeDtypeStruct((2, SLOTS, half, half), jnp.float32),
+        functools.partial(front_kernel, peers),
+        out_shape=(
+            jax.ShapeDtypeStruct(momentum.shape, jnp.float32),
+            jax.ShapeDtypeStruct((2, SLOTS, half, half), jnp.float32),
+            parts,
+            parts,
+        ),
+        in_specs=[anywhere, vmem],
+        out_specs=(anywhere, vmem, anywhere, anywhere),
         scratch_shapes=[
-            pltpu.VMEM((2 * count, tile, half), jnp.bfloat16),
-            pltpu.VMEM((2 * count, tile, half), jnp.bfloat16),
+            pltpu.VMEM((rows, width), jnp.float32),
+            pltpu.VMEM((rows, width), jnp.float32),
+            pltpu.VMEM((2, rows, half), jnp.float32),
+            pltpu.VMEM((3, 2, rows, half), jnp.float32),
+            pltpu.VMEM((4, 2, rows, half), jnp.bfloat16),
+            pltpu.VMEM((4, 2, rows, half), jnp.bfloat16),
+            pltpu.VMEM((9, half, half), jnp.float32),
+            pltpu.VMEM((9, peers - 1, slab, half), jnp.float32),
+            pltpu.VMEM((2, SLOTS, half, half), jnp.float32),
+            semaphores((PIECES,)),
+            semaphores((3, 4, 2)),
+            semaphores((PIECES,)),
+            semaphores((PIECES,)),
+            semaphores((3, 2, PIECES)),
+            semaphores((3, 2, PIECES)),
+            semaphores((9,)),
+            semaphores((9,)),
+            semaphores((9,)),
+            semaphores((9,)),
         ],
         compiler_params=pltpu.CompilerParams(
-            vmem_limit_bytes=VMEM_BYTES, dimension_semantics=("arbitrary",)
+            collective_id=1, has_side_effects=True, vmem_limit_bytes=VMEM_BYTES
         ),
         cost_estimate=pl.CostEstimate(
             flops=2 * 3 * 9 * rows * half * half,
-            bytes_accessed=4 * rows * count * width,
+            bytes_accessed=4 * rows * width * 8,
             transcendentals=0,
         ),
-    )(gathered)
+    )(grads, momentum)
 
 
 def iterate_kernel(
@@ -389,59 +662,49 @@
     )(share)
 
 
-def step_kernel(x_ref, high_ref, low_ref, out_ref):
-    width = x_ref.shape[-1]
+def step_kernel(x_high, x_low, high_ref, low_ref, out_ref):
+    place = lax.axis_index("tp")
+    half = x_high.shape[-1]
     total = None
-    for q in range(x_ref.shape[0]):
-        x_high, x_low = split(x_ref[q])
-        rows = slice(q * width, (q + 1) * width)
-        part = dot3(x_high, x_low, high_ref[rows, :], low_ref[rows, :])
-        total = part if total is None else total + part
-    out_ref[...] = total
-
-
-def step_of(gathered, high, low):
-    count, rows, width = gathered.shape
+    for s in range(4):
+        for side in range(2):
+            start = (2 * partner(place, s) + side) * half
+            rows = pl.ds(pl.multiple_of(start, half), half)
+            part = dot3(
+                x_high[s, side], x_low[s, side], high_ref[rows, :], low_ref[rows, :]
+            )
+            total = part if total is None else total + part
+    out_ref[0] = total
+
+
+def step_of(x_high, x_low, high, low):
+    count, sides, rows, half = x_high.shape
+    size, width = high.shape
     tile = min(rows, 256)
-    whole = pl.BlockSpec((count * width, width), lambda i: (0, 0))
+    piece = pl.BlockSpec((count, sides, tile, half), lambda i: (0, 0, i, 0))
+    whole = pl.BlockSpec((size, width), lambda i: (0, 0))
     return pl.pallas_call(
         step_kernel,
         grid=(rows // tile,),
-        in_specs=[
-            pl.BlockSpec((count, tile, width), lambda i: (0, i, 0)),
-            whole,
-            whole,
-        ],
-        out_specs=pl.BlockSpec((tile, width), lambda i: (i, 0)),
-        out_shape=jax.ShapeDtypeStruct((rows, width), jnp.float32),
+        in_specs=[piece, piece, whole, whole],
+        out_specs=pl.BlockSpec((1, tile, width), lambda i: (0, i, 0)),
+        out_shape=jax.ShapeDtypeStruct((1, rows, width), jnp.float32),
         compiler_params=pltpu.CompilerParams(
             vmem_limit_bytes=VMEM_BYTES, dimension_semantics=("arbitrary",)
         ),
         cost_estimate=pl.CostEstimate(
-            flops=2 * 3 * rows * count * width * width,
-            bytes_accessed=4 * rows * (count + 1) * width,
+            flops=2 * 3 * rows * size * width,
+            bytes_accessed=4 * rows * (size + width),
             transcendentals=0,
         ),
-    )(gathered, high, low)
-
-
-def orthogonalize(moment):
-    rows_count = moment.shape[0] * lax.axis_size("fs")
-    gathered = lax.all_gather(moment, "tp", axis=0, tiled=False)
-    share = gram_share(gathered)
-    shape = share.shape
-    share = share.reshape(-1, shape[-1])
-    share = lax.psum_scatter(share, "fs", scatter_dimension=0, tiled=True)
-    share = lax.all_gather(share, "fs", axis=0, tiled=True).reshape(shape)
+    )(x_high, x_low, high, low)
+
+
+def per_device(grads, momentum):
+    rows_count = momentum.shape[1] * lax.axis_size("fs")
+    moment, share, x_high, x_low = front(grads, momentum)
     high, low = polynomial(share, rows_count)
-    return step_of(gathered, high, low)
-
-
-def per_device(grads, momentum):
-    shares = lax.psum_scatter(grads[0], "rep", scatter_dimension=0, tiled=True)
-    moment = momentum_decay * momentum + shares
-    steps = [orthogonalize(moment[k]) for k in range(moment.shape[0])]
-    return (moment, jnp.stack(steps))
+    return (moment, step_of(x_high, x_low, high, low))
 
 
 def solution(mesh):

time: 675 us -> 542 us (0.80)
  waiting for transfers between devices: 289 us -> 0 us
  Pallas kernels: 359 us -> 528 us
  between operations: 14.2 us -> 1.09 us
    all_gather x2 -> x0, waiting for transfers between devices: 214 us -> none  [the longest x1 159 us: orthogonalize(): gathered = lax.all_gather(moment, 'tp', axis=0, tiled=False)]
    pallas_call x2, Pallas kernels: 33.8 us -> 206 us  [the longest x1 188 us: front(): pl.pallas_call(functools.partial(front_kernel, peers), out_shape=(jax.Sha...]
    reduce_scatter x2 -> x0, waiting for transfers between devices: 73.8 us -> none  [the longest x1 52.4 us: orthogonalize(): share = lax.psum_scatter(share, 'fs', scatter_dimension=0, tiled=True)]
  transfers between devices with their start and end apart: 4 -> 0, of which waited for: 4 -> 0; matrix products, arithmetic and copies ran while one was open for 0% -> 0% of each run, Pallas kernels for 0% -> 0%
where the time goes in v2:
time: 542 us; the launch traced here: 534 us
  Pallas kernels  528 us (97%)
    pallas_call x1, Pallas kernels, polynomial(): pl.pallas_call(functools.partial(iterate_kernel, rows_count), out_shape=(...  322 us
    pallas_call x1, Pallas kernels, front(): pl.pallas_call(functools.partial(front_kernel, peers), out_shape=(jax.Sha...  188 us
    pallas_call x1, Pallas kernels, step_of(): pl.pallas_call(step_kernel, grid=(rows // tile,), in_specs=[piece, piece,...  18.2 us

profile of v2, /device:TPU:0, one launch (start us, length us, event | category | flops | bytes accessed | tf_op | source)
XLA Modules:
  0.0 534.2 jit_solution(8375364380548573184)
XLA Ops:
  0.6 187.8 %shard_map.41 = (f32[1,2048,512]{2,1,0:T(8,128)}, f32[2,5,256,256]{3,2,1,0:T(8,128)}, bf16[4,2,2048,256]{3,2,1,0:T(8,128)(2,1)}, bf16[4,2,2048,256]{3,2,1,0:T(8,128)(2,1)}) custom-call(f32[1,2,2048,512]{3,2,1,0:T(8,128)} %grads_ref.1, f32[1,2048,512]{2,1,0:T(8,128)} %momentum_ref.1), custom_call_target="tpu_custom_call" | custom-call | flops 7247757312 | bytes 33554432 | tf_op jit(solution)/shard_map/pallas_call | solution.py:340
  188.5 322.4 %shard_map.42 = (bf16[2048,512]{1,0:T(8,128)(2,1)}, bf16[2048,512]{1,0:T(8,128)(2,1)}) custom-call(f32[2,5,256,256]{3,2,1,0:T(8,128)} %get-tuple-element.11.share_ref), custom_call_target="tpu_custom_call" | custom-call | flops 154618822656 | bytes 8388608 | tf_op jit(solution)/shard_map/pallas_call | solution.py:634
  510.9 18.2 %shard_map.43 = f32[1,2048,512]{2,1,0:T(8,128)} custom-call(bf16[4,2,2048,256]{3,2,1,0:T(8,128)(2,1)} %get-tuple-element.9.x_high, bf16[4,2,2048,256]{3,2,1,0:T(8,128)(2,1)} %get-tuple-element.10.x_low, bf16[2048,512]{1,0:T(8,128)(2,1)} %get-tuple-element.12.high_ref, bf16[2048,512]{1,0:T(8,128)(2,1)} %get-tuple-element.13.low_ref), custom_call_target="tpu_custom_call" | custom-call | flops 12884901888 | bytes 20971520 | tf_op jit(solution)/shard_map/pallas_call | solution.py:686
  529.1 4.6 copy.5

commit v3 on v2

--- a/solution.py
+++ b/solution.py
@@ -416,70 +416,83 @@
         rows = lax.broadcasted_iota(jnp.int32, shape, 0) + at * tile
         return lambda col: rows == lax.broadcasted_iota(jnp.int32, shape, 1) + col
 
+    layer = lax.axis_index("fs")
+    odd = lax.rem(layer, 2)
+    twin = layer + 1 - 2 * odd
+
+    def turn(chunk, slot):
+        return lax.rem(odd + slots(chunk).index(slot) + chunk, 2)
+
+    def slots(chunk):
+        return [k for k in range(SLOTS) if not (chunk == 1 and k == 1)]
+
+    def beside(way):
+        return (1 - way) * neighbours[1] + way * neighbours[2]
+
     def copy(via, chunk, slot):
+        way = turn(chunk, slot)
         if via == 0:
-            source, target, to = held.at[0, chunk, slot], held.at[1, chunk, slot], 1
+            source, target = held.at[0, chunk, slot], held.at[1 + way, chunk, slot]
         elif via == 1:
-            source, target, to = held.at[0, chunk, slot], held.at[2, chunk, slot], 2
-        elif over_y(chunk, slot):
-            source, target, to = held.at[1, chunk, slot], held.at[3, chunk, slot], 2
+            source, target = held.at[1 + way, chunk, slot], held.at[3, chunk, slot]
         else:
-            source, target, to = held.at[2, chunk, slot], held.at[3, chunk, slot], 1
+            source = target = held.at[1 + way, chunk, slot]
         return pltpu.make_async_remote_copy(
             src_ref=source,
             dst_ref=target,
             send_sem=send_sem.at[via, chunk, slot],
             recv_sem=recv_sem.at[via, chunk, slot],
-            device_id={"tp": neighbours[to]},
+            device_id={"fs": twin}
+            if via == 2
+            else {"tp": beside(way if via == 0 else 1 - way)},
             device_id_type=MESH,
         )
-
-    def over_y(chunk, slot):
-        order = [k for k in range(SLOTS) if not (chunk == 1 and k == 1)]
-        place_in = order.index(slot)
-        return place_in % 2 == chunk
-
-    def slots(chunk):
-        return [k for k in range(SLOTS) if not (chunk == 1 and k == 1)]
 
     def send(chunk, slot):
         copy(0, chunk, slot).start()
+
+    def relay(chunk, slot):
+        copy(0, chunk, slot).wait_recv()
         copy(1, chunk, slot).start()
-
-    def relay(chunk):
-        for slot in slots(chunk):
-            copy(0, chunk, slot).wait_recv()
-            copy(1, chunk, slot).wait_recv()
-            copy(2, chunk, slot).start()
-
-    def assemble(s, chunk):
-        q = partner(place, s)
+        copy(2, chunk, slot).start()
+
+    x, y = bits(place)
+
+    def place_block(s, chunk, slot):
+        across_y = s // 2
+        across_x = s - 2 * across_y
+        q = place + across_x * (1 - 2 * x) + across_y * (2 - 4 * y)
         col = 2 * q + chunk
-        for slot in slots(chunk):
-            row = block_row(q, chunk, slot)
-            value = held[s, chunk, slot]
-            high, low = split(value)
-            gram_high[rows_of(row), rows_of(col)] = high
-            gram_low[rows_of(row), rows_of(col)] = low
-            if slot > 0:
-                high, low = split(value.T)
-                gram_high[rows_of(col), rows_of(row)] = high
-                gram_low[rows_of(col), rows_of(row)] = low
+        row = block_row(q, chunk, slot)
+        value = held[s, chunk, slot]
+        high, low = split(value)
+        gram_high[rows_of(row), rows_of(col)] = high
+        gram_low[rows_of(row), rows_of(col)] = low
+        if slot > 0:
+            high, low = split(value.T)
+            gram_high[rows_of(col), rows_of(row)] = high
+            gram_low[rows_of(col), rows_of(row)] = low
+
+    def arrived(chunk, slot):
+        copy(1, chunk, slot).wait_recv()
+        copy(2, chunk, slot).wait_recv()
 
     def exchange(between):
-        relay(0)
         between()
-        assemble(0, 0)
-        assemble(0, 1)
-        for s in (1, 2):
-            assemble(s, 0)
-        relay(1)
-        for s in (1, 2):
-            assemble(s, 1)
-        for chunk in range(2):
-            for slot in slots(chunk):
-                copy(2, chunk, slot).wait_recv()
-            assemble(3, chunk)
+
+        def place_all(first_source, chunk, slot):
+            def body(s, _):
+                place_block(s, chunk, slot)
+                return 0
+
+            lax.fori_loop(first_source, 4, body, 0)
+
+        for slot in slots(0):
+            arrived(0, slot)
+            place_all(0, 0, slot)
+        for slot in slots(1):
+            arrived(1, slot)
+            place_all(0, 1, slot)
         for via in range(3):
             for chunk in range(2):
                 for slot in slots(chunk):
@@ -522,9 +535,12 @@
         lax.fori_loop(0, tiles, body, 0)
 
     def following(chunk, scale):
-        behind = None
-        for slot in slots(chunk):
-            row = block_row(place, chunk, slot)
+        order = slots(chunk)
+        blocks = [block_row(place, chunk, slot) for slot in order]
+
+        def body(at, _):
+            row = sum(jnp.where(at == k, blocks[k], 0) for k in range(len(order)))
+            slot = sum(jnp.where(at == k, order[k], 0) for k in range(len(order)))
             rows = rows_of(row)
             value = scale * times_gram(row, 1, op_high[0], op_low[0])
             held[0, chunk, slot] = (
@@ -532,12 +548,22 @@
                 + poly_cubic * second[rows, :]
                 + poly_quintic * value
             )
-            if behind is not None:
-                send(chunk, behind)
-            behind = slot
-        send(chunk, behind)
-
-    def apply(scale, finish):
+            for k in range(len(order) - 1):
+
+                @pl.when(at == k + 1)
+                def _():
+                    send(chunk, order[k])
+
+            return 0
+
+        lax.fori_loop(0, len(order), body, 0)
+        send(chunk, order[-1])
+
+    def relay_last():
+        for slot in slots(1):
+            relay(1, slot)
+
+    def apply(scale, finish, between=lambda: None):
         def body(at, _):
             rows = rows_of(2 * at, 2)
             part = times_gram(2 * at, 2, wide_high[0], wide_low[0])
@@ -549,6 +575,7 @@
             return 0
 
         lax.fori_loop(0, tiles, body, 0)
+        between()
 
         def body2(at, _):
             rows = rows_of(2 * at, 2)
@@ -565,15 +592,24 @@
         wide_low[0, rows, :] = low
 
     barrier = pltpu.get_barrier_semaphore()
-    for to in (1, 2):
+    def tell(semaphore):
+        for to in (1, 2):
+            pl.semaphore_signal(
+                semaphore, inc=1, device_id={"tp": neighbours[to]}, device_id_type=MESH
+            )
         pl.semaphore_signal(
-            barrier, inc=1, device_id={"tp": neighbours[to]}, device_id_type=MESH
-        )
+            semaphore, inc=1, device_id={"fs": twin}, device_id_type=MESH
+        )
+
+    tell(barrier)
     held[0] = share_ref[...]
-    pl.semaphore_wait(barrier, 2)
+    pl.semaphore_wait(barrier, 3)
     for chunk in range(2):
         for slot in slots(chunk):
             send(chunk, slot)
+    for slot in slots(0):
+        relay(0, slot)
+    relay_last()
     exchange(lambda: None)
 
     on_diagonal = lax.broadcasted_iota(
@@ -600,10 +636,7 @@
 
             apply(scale, finish)
             break
-        for to in (1, 2):
-            pl.semaphore_signal(
-                free_sem, inc=1, device_id={"tp": neighbours[to]}, device_id_type=MESH
-            )
+        tell(free_sem)
         for chunk in range(2):
 
             def also(rows, factor):
@@ -615,15 +648,24 @@
                     wide_low[0, rows, cols] = low
 
             sweep_factor(chunk, scale, also)
+            if chunk == 1:
+                relay(0, 0)
             times(0, 1, first, scale)
+            if chunk == 1:
+                relay(0, 1)
+                relay(0, 2)
             times(1, 0, second, scale)
+            if chunk == 1:
+                relay(0, 3)
+                relay(0, 4)
             if chunk == 0:
-                pl.semaphore_wait(free_sem, 2)
+                pl.semaphore_wait(free_sem, 3)
             following(chunk, scale)
         if sweep == 0:
+            relay_last()
             exchange(lambda: None)
         else:
-            exchange(lambda: apply(scale, keep_product))
+            exchange(lambda: apply(scale, keep_product, relay_last))
         scale = jnp.ones((1, 1), jnp.float32)
 
 

time: 542 us -> 487 us (0.90)
  Pallas kernels: 528 us -> 473 us
    pallas_call x1, Pallas kernels: 322 us -> 266 us  [polynomial(): pl.pallas_call(functools.partial(iterate_kernel, rows_count), out_shape=(...]
where the time goes in v3:
time: 487 us; the launch traced here: 478 us
  Pallas kernels  473 us (97%)
    pallas_call x1, Pallas kernels, polynomial(): pl.pallas_call(functools.partial(iterate_kernel, rows_count), out_shape=(...  266 us
    pallas_call x1, Pallas kernels, front(): pl.pallas_call(functools.partial(front_kernel, peers), out_shape=(jax.Sha...  188 us
    pallas_call x1, Pallas kernels, step_of(): pl.pallas_call(step_kernel, grid=(rows // tile,), in_specs=[piece, piece,...  18.2 us

profile of v3, /device:TPU:0, one launch (start us, length us, event | category | flops | bytes accessed | tf_op | source)
XLA Modules:
  0.0 478.3 jit_solution(14311826461684266753)
XLA Ops:
  0.6 187.8 %shard_map.41 = (f32[1,2048,512]{2,1,0:T(8,128)}, f32[2,5,256,256]{3,2,1,0:T(8,128)}, bf16[4,2,2048,256]{3,2,1,0:T(8,128)(2,1)}, bf16[4,2,2048,256]{3,2,1,0:T(8,128)(2,1)}) custom-call(f32[1,2,2048,512]{3,2,1,0:T(8,128)} %grads_ref.1, f32[1,2048,512]{2,1,0:T(8,128)} %momentum_ref.1), custom_call_target="tpu_custom_call" | custom-call | flops 7247757312 | bytes 33554432 | tf_op jit(solution)/shard_map/pallas_call | solution.py:340
  188.5 266.5 %shard_map.42 = (bf16[2048,512]{1,0:T(8,128)(2,1)}, bf16[2048,512]{1,0:T(8,128)(2,1)}) custom-call(f32[2,5,256,256]{3,2,1,0:T(8,128)} %get-tuple-element.11.share_ref), custom_call_target="tpu_custom_call" | custom-call | flops 154618822656 | bytes 8388608 | tf_op jit(solution)/shard_map/pallas_call | solution.py:676
  454.9 18.2 %shard_map.43 = f32[1,2048,512]{2,1,0:T(8,128)} custom-call(bf16[4,2,2048,256]{3,2,1,0:T(8,128)(2,1)} %get-tuple-element.9.x_high, bf16[4,2,2048,256]{3,2,1,0:T(8,128)(2,1)} %get-tuple-element.10.x_low, bf16[2048,512]{1,0:T(8,128)(2,1)} %get-tuple-element.12.high_ref, bf16[2048,512]{1,0:T(8,128)(2,1)} %get-tuple-element.13.low_ref), custom_call_target="tpu_custom_call" | custom-call | flops 12884901888 | bytes 20971520 | tf_op jit(solution)/shard_map/pallas_call | solution.py:728
  473.2 4.6 copy.5
